TPU v7x, 512 devices: a whole 4x8x8 slice. The times are simulated.
512 devices in a mesh: sp: 64 (over z, y), tp: 8 (over x, core).
Axes of the slice: x: 4, y: 8, z: 8, core: 2. Of those that a mesh axis runs over, the one named last changes fastest.
Arguments:
- query_one: bfloat16 [8192, 1024], P('sp', 'tp'), may hold values from -6 to 6
- key_one: bfloat16 [8192, 1024], P('sp', 'tp'), may hold values from -6 to 6
- query_two: bfloat16 [8192, 512], P('sp', 'tp'), may hold values from -6 to 6
- key_two: bfloat16 [8192, 512], P('sp', 'tp'), may hold values from -6 to 6
- values: bfloat16 [8192, 2048], P('sp', 'tp'), may hold values from -6 to 6
- out_gate: bfloat16 [8192, 2048], P('sp', 'tp'), may hold values from -6 to 6
- in_gate: float32 [16, 8192], P('tp', 'sp'), may hold values from -3 to 150
- forget_gate: float32 [16, 8192], P('tp', 'sp'), may hold values from -1 to 24
- head_gain: float32 [2048], P('tp'), may hold values from 0.1 to 1.9
- out_weight: bfloat16 [2048, 2048], P('tp'), may hold values from -0.125 to 0.125
- stream: bfloat16 [8192, 2048], P('sp'), may hold values from -6 to 6
- mix_gain: float32 [2048], replicated, may hold values from 0.1 to 1.9
- up_weight: bfloat16 [2048, 8192], P('sp', 'tp'), may hold values from -0.125 to 0.125
- down_weight: bfloat16 [8192, 2048], P('tp', 'sp'), may hold values from -0.0625 to 0.0625
- out_gain: float32 [2048], replicated, may hold values from 0.1 to 1.9
Outputs:
- result: bfloat16 [8192, 2048], P(('sp', 'tp'))
All inputs are finite; a program needn't handle non-finite values.
Results may differ from a plain program's by a relative error of at most 0.018.
Values may be sent and summed in bfloat16 or wider, within the bound.
A program may use at most 64 MiB of HBM per device.

v0:
```python
from functools import partial

import jax
import jax.numpy as jnp
from jax import lax
from jax.sharding import Mesh
from jax.sharding import PartitionSpec as P

BLOCK = 64
SP = ("sp_0", "sp_1")
SP_TP = ("sp_0", "sp_1", "tp")


NEG_BIG = -1e30
EPS = 1e-05


def neutral_like(value, identity):
    return jax.tree.map(
        lambda a, e: jnp.broadcast_to(jnp.asarray(e, a.dtype), a.shape), value, identity
    )


def prefix_by_axis(value, axes, combine, identity):
    before = start = neutral_like(value, identity)
    subtotal = value
    for axis in reversed(axes):
        length, position = (lax.axis_size(axis), lax.axis_index(axis))
        pieces = jax.tree.map(lambda part: lax.all_gather(part, axis), subtotal)
        inside, subtotal = (start, start)
        for k in range(length):
            passed = k < position
            subtotal = combine(subtotal, jax.tree.map(lambda part: part[k], pieces))
            inside = jax.tree.map(lambda new, old: jnp.where(passed, new, old), subtotal, inside)
        before = combine(inside, before)
    return before


def cut_along(value, dim, length):
    lengths = value.shape
    parts = value.reshape(*lengths[:dim], length, lengths[dim] // length, *lengths[dim + 1 :])
    return jnp.moveaxis(parts, dim, 0)


def summed_on_arrival(value, axis, dim):
    length = lax.axis_size(axis)
    parts = lax.all_to_all(cut_along(value, dim, length), axis, 0, 0, tiled=True)
    return jnp.sum(parts.astype(jnp.float32), axis=0)


def in_order(parts, dim):
    lengths = list(parts.shape[1:])
    lengths[dim] *= parts.shape[0]
    return jnp.moveaxis(parts, 0, dim).reshape(lengths)


def copy_for_each(value, axis):
    length = lax.axis_size(axis)
    return lax.all_to_all(
        jnp.broadcast_to(value[None], (length, *value.shape)), axis, 0, 0, tiled=True
    )


def collect(value, axis, dim):
    return in_order(copy_for_each(value, axis), dim)


def combine(earlier, later):
    decay_early, cell_early, norm_early, peak_early = earlier
    decay_late, cell_late, norm_late, peak_late = later
    ceiling = jnp.maximum(decay_late + peak_early, peak_late)
    keep_share = jnp.exp(decay_late + peak_early - ceiling)
    fresh_share = jnp.exp(peak_late - ceiling)
    cell_new = keep_share[..., None, None] * cell_early + fresh_share[..., None, None] * cell_late
    norm_new = keep_share[..., None] * norm_early + fresh_share[..., None] * norm_late
    return (decay_early + decay_late, cell_new, norm_new, ceiling)


def combine_groups(earlier, later):
    return (combine(earlier[0], later[0]), combine(earlier[1], later[1]))


def summarize(queries, keys_in, values_in, in_pre, forget_pre, block_len):
    length, width_k = queries.shape
    block_count = length // block_len
    scaled_keys = keys_in.astype(jnp.float32).reshape(
        block_count, block_len, width_k
    ) * width_k ** (-0.5)
    values_f = values_in.astype(jnp.float32).reshape(block_count, block_len, -1)
    width_v = values_f.shape[-1]
    log_forget = jax.nn.log_sigmoid(forget_pre).reshape(block_count, block_len)
    log_input = in_pre.reshape(block_count, block_len)
    cumulative = jnp.cumsum(log_forget, 1)
    decay_total = cumulative[:, -1]
    weight_log = decay_total[:, None] - cumulative + log_input
    peak_log = jnp.max(weight_log, 1)
    weighted = jnp.exp(weight_log - peak_log[:, None])[..., None] * scaled_keys
    cell_states = jnp.einsum("cld,cle->cde", weighted, values_f, precision=lax.Precision.HIGHEST)
    norm_states = jnp.sum(weighted, 1)
    identity = (
        jnp.zeros((), jnp.float32),
        jnp.zeros((width_k, width_v), jnp.float32),
        jnp.zeros((width_k,), jnp.float32),
        jnp.full((), NEG_BIG, jnp.float32),
    )

    def advance(running, element):
        return (combine(running, element), running)

    closing, prefix = lax.scan(advance, identity, (decay_total, cell_states, norm_states, peak_log))
    return (closing, prefix, (scaled_keys, values_f, cumulative, log_input))


def finish(queries, prefix, pieces, incoming):
    scaled_keys, values_f, cumulative, log_input = pieces
    block_count, block_len, width_k = scaled_keys.shape
    spread_in = jax.tree.map(
        lambda leaf: jnp.broadcast_to(leaf, (block_count,) + leaf.shape), incoming
    )
    _, cell_states, norm_states, peaks = combine(spread_in, prefix)
    query_f = queries.astype(jnp.float32).reshape(block_count, block_len, width_k)
    log_gaps = cumulative[:, :, None] - cumulative[:, None, :] + log_input[:, None, :]
    causal = jnp.arange(block_len)[:, None] >= jnp.arange(block_len)[None, :]
    log_gaps = jnp.where(causal[None], log_gaps, -jnp.inf)
    carried = cumulative + peaks[:, None]
    ceiling = jnp.maximum(carried, jnp.max(log_gaps, 2))
    scores = jnp.einsum("cld,csd->cls", query_f, scaled_keys, precision=lax.Precision.HIGHEST)
    scores = scores * jnp.exp(log_gaps - ceiling[..., None])
    carry_weight = jnp.exp(carried - ceiling)
    numerator = carry_weight[..., None] * jnp.einsum(
        "cld,cde->cle", query_f, cell_states, precision=lax.Precision.HIGHEST
    )
    numerator = numerator + jnp.einsum(
        "cls,cse->cle", scores, values_f, precision=lax.Precision.HIGHEST
    )
    denominator = carry_weight * jnp.einsum(
        "cld,cd->cl", query_f, norm_states, precision=lax.Precision.HIGHEST
    )
    denominator = denominator + jnp.sum(scores, 2)
    result = numerator / jnp.maximum(jnp.abs(denominator), jnp.exp(-ceiling))[..., None]
    return result.reshape(block_count * block_len, -1)


def head_norm(cell_out):
    center = jnp.mean(cell_out, -1, keepdims=True)
    spread = jnp.mean(jnp.square(cell_out - center), -1, keepdims=True)
    return (cell_out - center) * lax.rsqrt(spread + EPS)


def layer_norm(rows_f, gain):
    center = jnp.mean(rows_f, -1, keepdims=True)
    spread = jnp.mean(jnp.square(rows_f - center), -1, keepdims=True)
    return (rows_f - center) * lax.rsqrt(spread + EPS) * gain


def empty_state(head_pairs, width_k, width_v):
    return (
        jnp.zeros((head_pairs,), jnp.float32),
        jnp.zeros((head_pairs, width_k, width_v), jnp.float32),
        jnp.zeros((head_pairs, width_k), jnp.float32),
        jnp.full((head_pairs,), NEG_BIG, jnp.float32),
    )


def body(
    query_one,
    key_one,
    query_two,
    key_two,
    values,
    out_gate,
    in_gate,
    forget_gate,
    head_gain,
    out_weight,
    stream,
    mix_gain,
    up_weight,
    down_weight,
    out_gain,
):
    length = stream.shape[0]
    head_pairs = in_gate.shape[0] // 2
    width_v = values.shape[1] // (2 * head_pairs)

    def split_heads(array):
        return array.reshape(length, head_pairs, -1).transpose(1, 0, 2)

    values_split = values.reshape(length, head_pairs, 2, width_v).transpose(1, 2, 0, 3)
    input_rows = in_gate.reshape(head_pairs, 2, length)
    forget_rows = forget_gate.reshape(head_pairs, 2, length)
    summary = jax.vmap(partial(summarize, block_len=BLOCK))
    queries_one = split_heads(query_one)
    queries_two = split_heads(query_two)
    closing_one, prefix_one, pieces_one = summary(
        queries_one, split_heads(key_one), values_split[:, 0], input_rows[:, 0], forget_rows[:, 0]
    )
    closing_two, prefix_two, pieces_two = summary(
        queries_two, split_heads(key_two), values_split[:, 1], input_rows[:, 1], forget_rows[:, 1]
    )
    identity = (
        empty_state(head_pairs, queries_one.shape[2], width_v),
        empty_state(head_pairs, queries_two.shape[2], width_v),
    )
    incoming = prefix_by_axis((closing_one, closing_two), SP, combine_groups, identity)
    cell_one = jax.vmap(finish)(queries_one, prefix_one, pieces_one, incoming[0])
    cell_two = jax.vmap(finish)(queries_two, prefix_two, pieces_two, incoming[1])
    normed = jnp.stack([head_norm(cell_one), head_norm(cell_two)], 1)
    normed = normed.transpose(2, 0, 1, 3).reshape(length, 2 * head_pairs * width_v)
    mixed_heads = (normed * head_gain * jax.nn.sigmoid(out_gate.astype(jnp.float32))).astype(
        jnp.bfloat16
    )
    own_rows = length // lax.axis_size("tp")
    leading = lax.axis_index("tp") * own_rows
    up_full = lax.all_gather(up_weight, SP, axis=0, tiled=True)

    def expand(row_block):
        return jnp.square(
            jax.nn.relu(jnp.dot(row_block, up_full, preferred_element_type=jnp.float32))
        ).astype(jnp.bfloat16)

    row_block = mixed_heads
    summed = summed_on_arrival(
        jnp.dot(row_block, out_weight, preferred_element_type=jnp.float32).astype(jnp.bfloat16),
        "tp",
        0,
    )
    mixer_out = lax.optimization_barrier(summed.astype(jnp.bfloat16))
    stream_own = lax.dynamic_slice_in_dim(stream, leading, own_rows, 0)
    first_own = layer_norm(
        stream_own.astype(jnp.float32) + mixer_out.astype(jnp.float32), mix_gain
    ).astype(jnp.bfloat16)
    hidden = (lambda portion, offset: expand(portion))(collect(first_own, "tp", 0), jnp.int32(0))
    partial_sums = jnp.dot(
        hidden,
        lax.all_gather(down_weight, SP, axis=1, tiled=True),
        preferred_element_type=jnp.float32,
    )
    mlp_out = lax.optimization_barrier(
        summed_on_arrival(partial_sums.astype(jnp.bfloat16), "tp", 0).astype(jnp.bfloat16)
    )
    return layer_norm(first_own.astype(jnp.float32) + mlp_out.astype(jnp.float32), out_gain).astype(
        jnp.bfloat16
    )


def solution(mesh):
    split = Mesh(mesh.devices.reshape(8, 8, mesh.shape["tp"]), ("sp_0", "sp_1", "tp"))
    return jax.shard_map(
        body,
        mesh=split,
        in_specs=(
            P(SP, "tp"),
            P(SP, "tp"),
            P(SP, "tp"),
            P(SP, "tp"),
            P(SP, "tp"),
            P(SP, "tp"),
            P("tp", SP),
            P("tp", SP),
            P("tp"),
            P("tp", None),
            P(SP, None),
            P(),
            P(SP, "tp"),
            P("tp", SP),
            P(),
        ),
        out_specs=P(SP_TP, None),
        check_vma=False,
    )
```

profile of v0, /device:TPU:1, one launch (start us, length us, event | category | flops | bytes accessed | tf_op | source)
XLA Modules:
  0.0 401.7 jit_solution(530743618393407571)
XLA Ops:
  6.5 0.7 all-gather.17.cloned.1.call-update
  7.4 0.8 reshape.2365
  8.2 0.8 reshape.2367
  9.0 0.8 negate_reduce_fusion.1
  10.1 0.9 reshape.2360
  10.9 0.8 convert_element_type.50
  13.2 1.3 dynamic-slice
  15.0 0.4 convolution_bitcast_fusion
  15.4 6.6 %while.50 = (s32[]{:T(128)}, f32[1]{0:T(128)}, f32[1,128,128]{2,1,0:T(8,128)S(1)}, f32[1,128]{1,0:T(1,128)S(1)}, f32[1]{0:T(128)}, /*index=5*/f32[2,1]{0,1:T(1,1...) while((s32[]{:T(128)}, f32[1]{0:T(128)}, ...), condition=%wide.region_4.5_spmd.clone, body=%wide.region_3.4_spmd.clone.sunk | while | flops 82568 | bytes 330562 | solution.py:110
  15.4 0.6 constant_dynamic-slice_fusion.8
  18.7 0.6 constant_dynamic-slice_fusion.8
  22.0 0.7 dynamic-update-slice
  22.8 0.7 dynamic-update-slice.2
  23.7 6.9 %while.51 = (s32[]{:T(128)}, f32[1]{0:T(128)}, f32[1,64,128]{2,1,0:T(8,128)S(1)}, f32[1,64]{1,0:T(1,128)S(1)}, f32[1]{0:T(128)}, /*index=5*/f32[2,1]{0,1:T(1,128...) while((s32[]{:T(128)}, f32[1]{0:T(128)}, ...), condition=%wide.region_13.14_spmd.clone, body=%wide.region_12.13_spmd.clone.sunk | while | flops 41288 | bytes 165954 | solution.py:110
  23.7 0.7 constant_dynamic-slice_fusion.9
  27.1 0.7 constant_dynamic-slice_fusion.9
  30.6 0.7 dynamic-update-slice.4
  31.4 0.7 dynamic-update-slice.6
  32.1 14.8 %all-reduce.8 = (f32[8]{0:T(128)S(1)}, f32[8]{0:T(128)S(1)}, f32[8]{0:T(128)S(1)}, f32[8]{0:T(128)S(1)}) all-reduce(f32[8]{0:T(128)S(1)} %dynamic-update-slice.4, f32[8]{0:T(128)S(1)} %dynamic-update-slice.6, f32[8]{0:T(128)S(1)} %dynamic-update-slice, f32[8]{0:T(128)S(1)} %dynamic-update-slice.2), channel_id=8, replica_groups=mesh['sp_0'=8,'sp_1'=8,'tp'=8] {'sp_1'}, use_global_device_ids=true, to_apply=%add.4 | all-reduce | flops 32 | bytes 256
  46.9 0.6 fusion.169
  48.1 0.6 fusion.168
  55.4 0.6 slice_add_fusion.15
  56.0 1.3 fusion.162
  57.3 1.2 slice_add_fusion.9
  61.6 1.3 fusion.175
  64.1 1.3 dynamic-slice.1
  65.5 1.3 slice_add_fusion.8
  66.8 0.6 fusion.171
  67.9 0.7 fusion.170
  73.1 0.6 slice_add_fusion.7
  73.7 1.3 fusion.165
  74.9 1.3 slice_add_fusion.1
  76.8 1.3 slice_add_fusion
  78.1 1.4 dynamic-update-slice.3
  79.5 1.4 dynamic-update-slice.1
  82.2 1.2 fusion.172
  83.4 1.4 dynamic-update-slice.7
  84.8 1.4 dynamic-update-slice.5
  86.8 20.3 %all-reduce.9 = (f32[8]{0:T(128)S(1)}, f32[8]{0:T(128)S(1)}, f32[8]{0:T(128)S(1)}, f32[8]{0:T(128)S(1)}) all-reduce(f32[8]{0:T(128)S(1)} %dynamic-update-slice.5, f32[8]{0:T(128)S(1)} %dynamic-update-slice.7, f32[8]{0:T(128)S(1)} %dynamic-update-slice.1, f32[8]{0:T(128)S(1)} %dynamic-update-slice.3), channel_id=9, replica_groups=mesh['sp_0'=8,'sp_1'=8,'tp'=8] {'sp_0'}, use_global_device_ids=true, to_apply=%add.5 | all-reduce | flops 32 | bytes 256
  107.1 0.7 fusion.164
  108.4 0.7 fusion.163
  135.2 0.7 fusion.167
  136.4 0.7 fusion.166
  165.0 22.9 %all-gather.4 = f32[8,128,128]{2,1,0:T(8,128)S(1)} all-gather(f32[1,128,128]{2,1,0:T(8,128)S(1)} %get-tuple-element.157), channel_id=6, replica_groups=mesh['sp_0'=8,'sp_1'=8,'tp'=8] {'sp_1'}, dimensions={0}, use_global_device_ids=true | all-gather | bytes 589824 | tf_op jit(solution)/shard_map/all_gather | solution.py:29
  188.8 10.9 %all-gather.12 = f32[8,1,128]{2,1,0:T(1,128)S(1)} all-gather(f32[1,1,128]{2,1,0:T(1,128)S(1)} %bitcast.589), channel_id=7, replica_groups=mesh['sp_0'=8,'sp_1'=8,'tp'=8] {'sp_1'}, dimensions={0}, use_global_device_ids=true | all-gather | bytes 4608 | tf_op jit(solution)/shard_map/all_gather | solution.py:29
  199.7 9.8 %all_gather.107 = f32[8,1,128]{2,1,0:T(1,128)S(1)} all-gather(f32[1,1,128]{2,1,0:T(1,128)S(1)} %get-tuple-element.425), channel_id=1, replica_groups=mesh['sp_0'=8,'sp_1'=8,'tp'=8] {'sp_0'}, dimensions={0}, use_global_device_ids=true | all-gather | bytes 4608 | tf_op jit(solution)/shard_map/all_gather | solution.py:29
  210.5 18.9 %all_gather.104 = f32[8,1,128,128]{3,2,1,0:T(8,128)S(1)} all-gather(f32[1,1,128,128]{3,2,1,0:T(8,128)S(1)} %bitcast_add_fusion.5), channel_id=1, replica_groups=mesh['sp_0'=8,'sp_1'=8,'tp'=8] {'sp_0'}, dimensions={0}, use_global_device_ids=true | all-gather | bytes 589824 | tf_op jit(solution)/shard_map/all_gather | solution.py:29
  229.5 0.3 fusion.13
  229.8 0.3 fusion.177
  239.4 10.7 %all-gather.13 = f32[8,1,64]{2,1,0:T(1,128)S(1)} all-gather(f32[1,1,64]{2,1,0:T(1,128)S(1)} %bitcast.588), channel_id=13, replica_groups=mesh['sp_0'=8,'sp_1'=8,'tp'=8] {'sp_1'}, dimensions={0}, use_global_device_ids=true | all-gather | bytes 2304 | tf_op jit(solution)/shard_map/all_gather | solution.py:29
  250.1 11.3 %all_gather.121 = f32[8,1,64]{2,1,0:T(1,128)S(1)} all-gather(f32[1,1,64]{2,1,0:T(1,128)S(1)} %get-tuple-element.433), channel_id=1, replica_groups=mesh['sp_0'=8,'sp_1'=8,'tp'=8] {'sp_0'}, dimensions={0}, use_global_device_ids=true | all-gather | bytes 2304 | tf_op jit(solution)/shard_map/all_gather | solution.py:29
  261.4 18.4 %all-gather.10 = f32[8,64,128]{2,1,0:T(8,128)S(1)} all-gather(f32[1,64,128]{2,1,0:T(8,128)S(1)} %get-tuple-element.165), channel_id=12, replica_groups=mesh['sp_0'=8,'sp_1'=8,'tp'=8] {'sp_1'}, dimensions={0}, use_global_device_ids=true | all-gather | bytes 294912 | tf_op jit(solution)/shard_map/all_gather | solution.py:29
  279.8 18.9 %all_gather.118 = f32[8,1,64,128]{3,2,1,0:T(8,128)S(1)} all-gather(f32[1,1,64,128]{3,2,1,0:T(8,128)S(1)} %bitcast_add_fusion.11), channel_id=1, replica_groups=mesh['sp_0'=8,'sp_1'=8,'tp'=8] {'sp_0'}, dimensions={0}, use_global_device_ids=true | all-gather | bytes 294912 | tf_op jit(solution)/shard_map/all_gather | solution.py:29
  299.7 0.3 fusion.174
  300.8 1.2 convolution_convert_fusion.1
  302.0 48.2 %all-to-all-start = ((bf16[8,16,2048]{2,1,0:T(8,128)(2,1)}), bf16[8,16,2048]{2,1,0:T(8,128)(2,1)S(1)}, u32[]{:S(2)}, u32[]{:S(2)}) async-start(bf16[8,16,2048]{2,1,0:T(8,128)(2,1)} %bitcast.185), calls=%async_computation | async-start | bytes 1048576 | tf_op jit(solution)/shard_map/all_to_all | solution.py:47
  350.2 9.3 %all-to-all-done = bf16[8,16,2048]{2,1,0:T(8,128)(2,1)S(1)} async-done(((bf16[8,16,2048]{2,1,0:T(8,128)(2,1)}), bf16[8,16,2048]{2,1,0:T(8,128)(2,1)S(1)}, u32[]{:S(2)}, u32[]{:S(2)}) %all-to-all-start) | async-done | bytes 524320 | tf_op jit(solution)/shard_map/all_to_all | solution.py:47
  359.6 1.0 fusion.21
  360.6 1.0 multiply_reduce_fusion.1
  361.6 0.9 multiply_convert_fusion.1
  362.6 12.7 %all_to_all.15 = bf16[8,16,2048]{2,1,0:T(8,128)(2,1)S(1)} all-to-all(bf16[8,16,2048]{2,1,0:T(8,128)(2,1)S(1)} %broadcast_in_dim.94), channel_id=1, replica_groups=mesh['sp_0'=8,'sp_1'=8,'tp'=8] {'tp'}, dimensions={0} | all-to-all | bytes 1048576 | tf_op jit(solution)/shard_map/all_to_all | solution.py:59
  375.3 5.6 %convolution_convert_fusion = bf16[128,2048]{1,0:T(8,128)(2,1)S(1)} fusion(bf16[1024,2048]{0,1:T(8,128)(2,1)} %all-gather.19.cloned.1.call-done, bf16[128,2048]{1,0:T(8,128)(2,1)S(1)} %bitcast.574, bf16[2048,1024]{1,0:T(8,128)(2,1)} %all-gather.17.cloned.1.call-done), kind=kOutput, calls=%fused_computation.20 | convolution fusion | flops 1074397184 | bytes 9437184 | tf_op jit(solution)/shard_map/dot_general | solution.py:234
  380.9 12.8 %all_to_all.16 = bf16[8,16,2048]{2,1,0:T(8,128)(2,1)S(1)} all-to-all(bf16[8,16,2048]{2,1,0:T(8,128)(2,1)S(1)} %bitcast.575), channel_id=1, replica_groups=mesh['sp_0'=8,'sp_1'=8,'tp'=8] {'tp'}, dimensions={0} | all-to-all | bytes 1048576 | tf_op jit(solution)/shard_map/all_to_all | solution.py:47
  394.1 0.7 multiply_convert_fusion
  (136 shorter events, 7.3 us)
Async XLA Ops:
  6.5 294.2 %copy-start = (bf16[256,2048]{1,0:T(8,128)(2,1)S(1)}, bf16[256,2048]{1,0:T(8,128)(2,1)}, u32[]{:S(2)}) copy-start(bf16[256,2048]{1,0:T(8,128)(2,1)} %param.28) | copy-start | bytes 3145732
  6.5 203.5 %copy-start.2 = (bf16[128,128]{1,0:T(8,128)(2,1)S(1)}, bf16[128,128]{1,0:T(8,128)(2,1)}, u32[]{:S(2)}) copy-start(bf16[128,128]{1,0:T(8,128)(2,1)} %param.19) | copy-start | bytes 98308
  6.5 368.8 %all-gather.17.cloned.1.call-start = ((), (), s32[]{:S(2)}) async-start(), calls=%async_computation.3 | async-start | bytes 4259840 | tf_op jit(solution)/shard_map/all_gather | solution.py:215
  7.3 368.1 %all-gather.19.cloned.1.call-start = ((), (), s32[]{:S(2)}) async-start(), calls=%async_computation.4 | async-start | bytes 4259840 | tf_op jit(solution)/shard_map/all_gather | solution.py:236
  15.4 223.9 %copy-start.3 = (bf16[128,64]{0,1:T(8,128)(2,1)S(1)}, bf16[128,64]{0,1:T(8,128)(2,1)}, u32[]{:S(2)}) copy-start(bf16[128,64]{0,1:T(8,128)(2,1)} %param.21) | copy-start | bytes 49156
  32.1 268.6 %copy-start.1 = (bf16[128,256]{1,0:T(8,128)(2,1)S(1)}, bf16[128,256]{1,0:T(8,128)(2,1)}, u32[]{:S(2)}) copy-start(bf16[128,256]{1,0:T(8,128)(2,1)} %param.24) | copy-start | bytes 196612
  32.1 268.6 %copy-start.6 = (f32[256]{0:T(256)S(1)}, f32[256]{0:T(256)}, u32[]{:S(2)}) copy-start(f32[256]{0:T(256)} %param.27) | copy-start | bytes 3076
  229.4 132.3 %copy-start.4 = (f32[2048]{0:T(1024)S(1)}, f32[2048]{0:T(1024)}, u32[]{:S(2)}) copy-start(f32[2048]{0:T(1024)} %param.30) | copy-start | bytes 24580
  302.0 57.6 %all-to-all-start = ((bf16[8,16,2048]{2,1,0:T(8,128)(2,1)}), bf16[8,16,2048]{2,1,0:T(8,128)(2,1)S(1)}, u32[]{:S(2)}, u32[]{:S(2)}) async-start(bf16[8,16,2048]{2,1,0:T(8,128)(2,1)} %bitcast.185), calls=%async_computation | async-start | bytes 1048576 | tf_op jit(solution)/shard_map/all_to_all | solution.py:47
  375.3 18.8 %copy-start.5 = (f32[2048]{0:T(1024)S(1)}, f32[2048]{0:T(1024)}, u32[]{:S(2)}) copy-start(f32[2048]{0:T(1024)} %param.33) | copy-start | bytes 24580
Sparse Core Ops, SparseCore 0:
  10.4 88.0 all-gather.16
  101.5 84.8 all-gather.18
where the time goes:
time: 404 us; the launch traced here: 402 us
  blocking collectives  182 us (45%)
  between operations  97.8 us (24%)
  starting transfers between devices  48.2 us (12%)
  local copies, waits for them, and re-layouts  23.7 us (6%)
  other arithmetic  20.4 us (5%)
  loops' own time  10.2 us (3%)
  waiting for transfers between devices  10.1 us (2%)
  matrix products  9.1 us (2%)
    all_gather x8, blocking collectives, prefix_by_axis(): pieces = jax.tree.map(lambda part: lax.all_gather(part, axis), subtotal)  122 us
    all_to_all x1, starting transfers between devices, summed_on_arrival(): lax.all_to_all(cut_along(value, dim, length), axis, 0, 0, tiled=True)  48.2 us
    unnamed x2, blocking collectives  35.1 us
    all_to_all x1, blocking collectives, summed_on_arrival(): lax.all_to_all(cut_along(value, dim, length), axis, 0, 0, tiled=True)  12.8 us
    all_to_all x1, blocking collectives, copy_for_each(): lax.all_to_all(jnp.broadcast_to(value[None], (length, *value.shape)), axi...  12.7 us
    unnamed x33, local copies, waits for them, and re-layouts  11.2 us
    another operation x2, loops' own time, summarize(): lax.scan(advance, identity, (decay_total, cell_states, norm_states, peak_...  10.2 us
    all_to_all x1, waiting for transfers between devices, summed_on_arrival(): lax.all_to_all(cut_along(value, dim, length), axis, 0, 0, tiled=True)  9.35 us
  transfers between devices with their start and end apart: 3, of which 1 were waited for; matrix products, arithmetic and copies ran while one was open for 12% of the time, Pallas kernels for 0%

commit v1 on v0

v1 whole, which is shorter than its diff:
```python
import functools

import jax
import jax.numpy as jnp
from jax import lax
from jax.experimental import pallas as pl
from jax.experimental.pallas import tpu as pltpu
from jax.sharding import Mesh
from jax.sharding import PartitionSpec as P

NEG_BIG = -1e30
EPS = 1e-05
META = 8
f32, bf16 = jnp.float32, jnp.bfloat16
MESH = pl.DeviceIdType.MESH


def dg(a, b, ca, cb):
    return lax.dot_general(a, b, (((ca,), (cb,)), ((), ())), preferred_element_type=f32)


def three(a):
    hi = a.astype(bf16)
    rest = a - hi.astype(f32)
    mid = rest.astype(bf16)
    return hi, mid, (rest - mid.astype(f32)).astype(bf16)


def left_dot(a, b, ca, cb):
    hi, mid, lo = three(a)
    return dg(hi, b, ca, cb) + (dg(mid, b, ca, cb) + dg(lo, b, ca, cb))


def right_dot(a, b, ca, cb):
    hi, mid, lo = three(b)
    return dg(a, hi, ca, cb) + (dg(a, mid, ca, cb) + dg(a, lo, ca, cb))


def remote(src, dst, ssem, rsem, target):
    return pltpu.make_async_remote_copy(
        src_ref=src, dst_ref=dst, send_sem=ssem, recv_sem=rsem, device_id=target, device_id_type=MESH
    )


class Ring:
    def __init__(self, axis, n, block, half, ssem, rsem):
        self.axis, self.n, self.block, self.half = axis, n, block, half
        self.ssem, self.rsem = ssem, rsem
        self.me = lax.axis_index(axis)
        self.steps = n // 2
        self.taken = set()

    def part(self, way, step, distance):
        away = self.n - distance if way == 0 else distance
        index = lax.rem(self.me + away, self.n)
        return self.block(index) if step < self.steps else self.half(index, way)

    def copy(self, way, step, distance):
        ref = self.part(way, step, distance)
        target = lax.rem(self.me + (1 if way == 0 else self.n - 1), self.n)
        return remote(
            ref, ref, self.ssem.at[way, step - 1], self.rsem.at[way, step - 1], {self.axis: target}
        )

    def send(self, step):
        if step <= self.steps:
            for way in (0, 1):
                self.copy(way, step, step - 1).start()

    def take(self, step):
        if 1 <= step <= self.steps and step not in self.taken:
            self.taken.add(step)
            for way in (0, 1):
                self.copy(way, step, step).wait_recv()

    def advance(self, step):
        self.take(step - 1)
        self.send(step)

    def drain(self):
        for step in range(1, self.steps + 1):
            for way in (0, 1):
                self.copy(way, step, step - 1).wait_send()


class Direct:
    def __init__(self, axis, n, source, slots, ssem, rsem):
        self.axis, self.n, self.source, self.slots = axis, n, source, slots
        self.ssem, self.rsem = ssem, rsem
        self.me = lax.axis_index(axis)

    def copy(self, d, slot):
        peer = lax.rem(self.me + d, self.n)
        return remote(
            self.source(peer), self.slots(slot), self.ssem.at[d], self.rsem.at[d], {self.axis: peer}
        )

    def send(self):
        for d in range(1, self.n):
            self.copy(d, self.me).start()

    def take(self):
        for d in range(1, self.n):
            self.copy(d, lax.rem(self.me + self.n - d, self.n)).wait_recv()

    def drain(self):
        for d in range(1, self.n):
            self.copy(d, self.me).wait_send()


def normed(rows, gain):
    center = jnp.mean(rows, -1, keepdims=True)
    away = rows - center
    spread = jnp.mean(away * away, -1, keepdims=True)
    return away * lax.rsqrt(spread + EPS) * gain


def kernel(
    sizes,
    q1_ref, k1_ref, q2_ref, k2_ref, v_ref, og_ref, ig_ref, fg_ref, hg_ref, ow_ref,
    stream_ref, mg_ref, up_ref, down_ref, outg_ref,
    out_ref,
    up_all, down_all, st_send, e1, e2_send, e2, f_send, cin,
    rs_send, rs1, x_all, hidden, rs2_send, rs2, stream_own,
    local_sem, ysend, yrecv, zsend, zrecv, bsend, brecv,
    p1send, p1recv, p2send, p2recv, tsend, trecv,
):
    NZ, NY, TP = sizes
    iz, iy, it = lax.axis_index("z"), lax.axis_index("y"), lax.axis_index("tp")
    T, KA = q1_ref.shape
    KB = k2_ref.shape[1]
    DV = v_ref.shape[1] // 2
    KEYS = KA + KB
    SH = KEYS // NY
    OWN = T // TP
    D = ow_ref.shape[1]
    RW = up_ref.shape[0]
    FD = up_ref.shape[1]

    barrier = pltpu.get_barrier_semaphore()
    peers = 0
    for axis, n in (("y", NY), ("z", NZ), ("tp", TP)):
        for d in range(1, n):
            peer = lax.rem(lax.axis_index(axis) + d, n)
            pl.semaphore_signal(barrier, inc=1, device_id={axis: peer}, device_id_type=MESH)
            peers += 1

    up_copy = pltpu.make_async_copy(up_ref, up_all.at[iz, iy], local_sem.at[0])
    down_copy = pltpu.make_async_copy(down_ref, down_all.at[iz, iy], local_sem.at[1])
    stream_copy = pltpu.make_async_copy(
        stream_ref.at[pl.ds(pl.multiple_of(it * OWN, OWN), OWN), :], stream_own, local_sem.at[2]
    )
    up_copy.start()
    down_copy.start()
    stream_copy.start()

    row_i = lax.broadcasted_iota(jnp.int32, (T, T), 0)
    col_i = lax.broadcasted_iota(jnp.int32, (T, T), 1)
    upto = jnp.where(row_i <= col_i, 1.0, 0.0).astype(bf16)
    log_forget = -jnp.log1p(jnp.exp(-fg_ref[...]))
    ig = ig_ref[...]
    cum = left_dot(log_forget, upto, 1, 0)
    total = cum[:, T - 1 : T]
    weight_log = total - cum + ig
    peak = jnp.max(weight_log, axis=1, keepdims=True)
    weight = jnp.exp(weight_log - peak)
    turned = jnp.transpose(jnp.concatenate([cum, weight, cum, weight], axis=0))
    weighted1 = turned[:, 2:3] * (k1_ref[...].astype(f32) * (KA ** -0.5))
    weighted2 = turned[:, 3:4] * (k2_ref[...].astype(f32) * (KB ** -0.5))
    v1, v2 = v_ref[:, :DV], v_ref[:, DV:]
    state = jnp.concatenate(
        [left_dot(weighted1, v1, 0, 0), left_dot(weighted2, v2, 0, 0)], axis=0
    )
    n1 = jnp.sum(weighted1, axis=0, keepdims=True)
    n2 = jnp.sum(weighted2, axis=0, keepdims=True)
    n2 = jnp.concatenate([n2, jnp.zeros((1, KA - KB), f32)], axis=1)
    ones = jnp.ones((1, KA), f32)
    meta = jnp.concatenate(
        [n1, n2, total * ones, peak * ones, jnp.zeros((META - 6, KA), f32)], axis=0
    )
    for j in range(NY):
        st_send[j, :SH] = state[j * SH : (j + 1) * SH]
        st_send[j, SH:] = meta
    e1[pl.ds(iy, 1)] = st_send[pl.ds(iy, 1)]

    pl.semaphore_wait(barrier, peers)

    first_hop = Direct("y", NY, lambda j: st_send.at[j], lambda s: e1.at[s], ysend, yrecv)
    first_hop.send()

    rows = RW // 2
    up1 = Ring("y", NY, lambda b: up_all.at[iz, b],
               lambda b, h: up_all.at[iz, b, h * rows : (h + 1) * rows], p1send.at[0], p1recv.at[0])
    down1 = Ring("z", NZ, lambda b: down_all.at[b, iy],
                 lambda b, h: down_all.at[b, iy, h * rows : (h + 1) * rows], p1send.at[1], p1recv.at[1])
    hy, hz = max(NY // 2, 1), max(NZ // 2, 1)
    up2 = Ring("z", NZ, lambda b: up_all.at[b],
               lambda b, h: up_all.at[b, h * hy : (h + 1) * hy], p2send.at[0], p2recv.at[0])
    down2 = Ring("y", NY, lambda b: down_all.at[:, b],
                 lambda b, h: down_all.at[h * hz : (h + 1) * hz, b], p2send.at[1], p2recv.at[1])

    up_copy.wait()
    down_copy.wait()
    up1.send(1)
    down1.send(1)

    causal = row_i >= col_i
    local = []
    for h, (q_ref, k_ref, vh) in enumerate(((q1_ref, k1_ref, v1), (q2_ref, k2_ref, v2))):
        gaps = turned[:, h : h + 1] - cum[h : h + 1] + ig[h : h + 1]
        gaps = jnp.where(causal, gaps, -jnp.inf)
        top = jnp.max(gaps, axis=1, keepdims=True)
        scores = dg(q_ref[...], k_ref[...], 1, 1) * (k_ref.shape[1] ** -0.5)
        scores = scores * jnp.exp(gaps - top)
        local.append((top, left_dot(scores, vh, 1, 0), jnp.sum(scores, axis=1, keepdims=True)))

    up1.advance(2)
    down1.advance(2)

    key_row = lax.broadcasted_iota(jnp.int32, (SH, KA), 0) + iy * SH

    def spread(pair):
        return jnp.where(key_row < KA, pair[0:1], pair[1:2])

    def combine(early, late):
        decay_e, cell_e, norm_e, peak_e = early
        decay_l, cell_l, norm_l, peak_l = late
        moved = decay_l + peak_e
        ceiling = jnp.maximum(moved, peak_l)
        keep, fresh = jnp.exp(moved - ceiling), jnp.exp(peak_l - ceiling)
        return (
            decay_e + decay_l,
            spread(keep) * cell_e + spread(fresh) * cell_l,
            keep * norm_e + fresh * norm_l,
            ceiling,
        )

    def loaded(ref, j):
        return (ref[j, SH + 2 : SH + 4], ref[j, :SH], ref[j, SH : SH + 2], ref[j, SH + 4 : SH + 6])

    nothing = (
        jnp.zeros((2, KA), f32), jnp.zeros((SH, DV), f32), jnp.zeros((2, KA), f32),
        jnp.full((2, KA), NEG_BIG, f32),
    )
    first_hop.take()
    running, inside = nothing, []
    for j in range(NY):
        inside.append(running)
        running = combine(running, loaded(e1, j))
    e2_send[:SH] = running[1]
    e2_send[SH:] = jnp.concatenate(
        [running[2], running[0], running[3], jnp.zeros((META - 6, KA), f32)], axis=0
    )
    e2[pl.ds(iz, 1)] = e2_send[...][None]
    second_hop = Direct("z", NZ, lambda j: e2_send, lambda s: e2.at[s], zsend, zrecv)
    second_hop.send()
    up1.advance(3)
    down1.advance(3)
    up1.advance(4)
    down1.advance(4)
    second_hop.take()
    before = nothing
    for k in range(NZ):
        later = combine(before, loaded(e2, k))
        before = jax.tree.map(lambda new, old: jnp.where(k < iz, new, old), later, before)
    norm_in, peak_in = jnp.zeros((2, KA), f32), jnp.zeros((2, KA), f32)
    for j in range(NY):
        _, cell_j, norm_j, peak_j = combine(before, inside[j])
        f_send[j] = cell_j
        norm_in = jnp.where(iy == j, norm_j, norm_in)
        peak_in = jnp.where(iy == j, peak_j, peak_in)
    cin[pl.ds(iy, 1)] = f_send[pl.ds(iy, 1)]
    third_hop = Direct("y", NY, lambda j: f_send.at[j], lambda s: cin.at[s], bsend, brecv)
    third_hop.send()
    up1.take(up1.steps)
    down1.take(down1.steps)
    up2.send(1)
    down2.send(1)
    third_hop.take()

    cell_in = cin[...].reshape(KEYS, DV)
    columns = []
    for h, (q_ref, cell) in enumerate(((q1_ref, cell_in[:KA]), (q2_ref, cell_in[KA:]))):
        q = q_ref[...]
        width = q.shape[1]
        top, own_num, own_den = local[h]
        carried = turned[:, h : h + 1] + peak_in[h : h + 1, 0:1]
        ceiling = jnp.maximum(carried, top)
        keep, fresh = jnp.exp(carried - ceiling), jnp.exp(top - ceiling)
        num = keep * right_dot(q, cell, 1, 0) + fresh * own_num
        den = keep * jnp.sum(q.astype(f32) * norm_in[h : h + 1, :width], axis=1, keepdims=True)
        den = den + fresh * own_den
        cell_out = num / jnp.maximum(jnp.abs(den), jnp.exp(-ceiling))
        center = jnp.mean(cell_out, -1, keepdims=True)
        away = cell_out - center
        var = jnp.mean(away * away, -1, keepdims=True)
        columns.append(away * lax.rsqrt(var + EPS))
    gate = 1.0 / (1.0 + jnp.exp(-og_ref[...].astype(f32)))
    mixed = (jnp.concatenate(columns, axis=1) * hg_ref[...] * gate).astype(bf16)
    wide = min(D, 512)
    for c in range(0, D, wide):
        part = dg(mixed, ow_ref[:, c : c + wide], 1, 0).astype(bf16)
        rs_send[:, :, c : c + wide] = part.reshape(TP, OWN, wide)
    rs1[pl.ds(it, 1)] = rs_send[pl.ds(it, 1)]
    out_proj = Direct("tp", TP, lambda j: rs_send.at[j], lambda s: rs1.at[s], tsend.at[0], trecv.at[0])
    out_proj.send()
    up2.advance(2)
    down2.advance(2)
    stream_copy.wait()
    out_proj.take()
    mixer = jnp.sum(rs1[...].astype(f32), axis=0).astype(bf16).astype(f32)
    first = normed(stream_own[...].astype(f32) + mixer, mg_ref[...]).astype(bf16)
    x_all[pl.ds(it, 1)] = first[None]
    rows_out = Direct("tp", TP, lambda j: x_all.at[it], lambda s: x_all.at[s], tsend.at[1], trecv.at[1])
    rows_out.send()
    up2.advance(3)
    down2.advance(3)
    rows_out.take()
    up2.advance(4)
    down2.advance(4)
    up2.take(up2.steps)

    wide_f = min(FD, 256)
    for c in range(0, FD, wide_f):
        x = x_all[...].reshape(T, D)
        w = up_all[:, :, :, c : c + wide_f].reshape(D, wide_f)
        act = jnp.maximum(dg(x, w, 1, 0), 0.0)
        hidden[:, c : c + wide_f] = (act * act).astype(bf16)
    down2.take(down2.steps)
    wide_d = NY * RW
    for z in range(NZ):
        w = down_all[z].reshape(wide_d, FD)
        part = dg(hidden[...], w, 1, 1).astype(bf16)
        rs2_send[:, :, z * wide_d : (z + 1) * wide_d] = part.reshape(TP, OWN, wide_d)
    rs2[pl.ds(it, 1)] = rs2_send[pl.ds(it, 1)]
    mlp = Direct("tp", TP, lambda j: rs2_send.at[j], lambda s: rs2.at[s], tsend.at[2], trecv.at[2])
    mlp.send()
    for item in (first_hop, second_hop, third_hop, out_proj, rows_out, up1, down1, up2, down2):
        item.drain()
    mlp.take()
    mlp_out = jnp.sum(rs2[...].astype(f32), axis=0).astype(bf16).astype(f32)
    base = x_all[pl.ds(it, 1)].reshape(OWN, D).astype(f32)
    out_ref[...] = normed(base + mlp_out, outg_ref[...]).astype(bf16)
    mlp.drain()


def layer(
    sizes, query_one, key_one, query_two, key_two, values, out_gate, in_gate, forget_gate,
    head_gain, out_weight, stream, mix_gain, up_weight, down_weight, out_gain,
):
    NZ, NY, TP = sizes
    T, D = stream.shape
    OWN = T // TP
    RW, FD = up_weight.shape
    SH = (query_one.shape[1] + query_two.shape[1]) // NY
    KA = query_one.shape[1]
    sem = pltpu.SemaphoreType.DMA
    half = max(NY, NZ) // 2
    vmem, hbm = pl.BlockSpec(memory_space=pltpu.VMEM), pl.BlockSpec(memory_space=pl.ANY)
    return pl.pallas_call(
        functools.partial(kernel, sizes),
        out_shape=jax.ShapeDtypeStruct((OWN, D), bf16),
        in_specs=[vmem] * 10 + [hbm, vmem, hbm, hbm, vmem],
        out_specs=vmem,
        scratch_shapes=[
            pltpu.VMEM((NZ, NY, RW, FD), bf16),
            pltpu.VMEM((NZ, NY, RW, FD), bf16),
            pltpu.VMEM((NY, SH + META, KA), f32),
            pltpu.VMEM((NY, SH + META, KA), f32),
            pltpu.VMEM((SH + META, KA), f32),
            pltpu.VMEM((NZ, SH + META, KA), f32),
            pltpu.VMEM((NY, SH, KA), f32),
            pltpu.VMEM((NY, SH, KA), f32),
            pltpu.VMEM((TP, OWN, D), bf16),
            pltpu.VMEM((TP, OWN, D), bf16),
            pltpu.VMEM((TP, OWN, D), bf16),
            pltpu.VMEM((T, FD), bf16),
            pltpu.VMEM((TP, OWN, D), bf16),
            pltpu.VMEM((TP, OWN, D), bf16),
            pltpu.VMEM((OWN, D), bf16),
            sem((3,)),
            sem((NY,)), sem((NY,)), sem((NZ,)), sem((NZ,)), sem((NY,)), sem((NY,)),
            sem((2, 2, half)), sem((2, 2, half)), sem((2, 2, half)), sem((2, 2, half)),
            sem((3, TP)), sem((3, TP)),
        ],
        compiler_params=pltpu.CompilerParams(
            collective_id=0, has_side_effects=True, vmem_limit_bytes=40 * 1024 * 1024
        ),
    )(
        query_one, key_one, query_two, key_two, values, out_gate, in_gate, forget_gate,
        head_gain.reshape(1, -1), out_weight, stream, mix_gain.reshape(1, -1), up_weight,
        down_weight.T, out_gain.reshape(1, -1),
    )


def build(mesh, nz, ny):
    tp = mesh.shape["tp"]
    split = Mesh(mesh.devices.reshape(nz, ny, tp), ("z", "y", "tp"))
    SP = ("z", "y")
    return jax.shard_map(
        functools.partial(layer, (nz, ny, tp)),
        mesh=split,
        in_specs=(
            P(SP, "tp"), P(SP, "tp"), P(SP, "tp"), P(SP, "tp"), P(SP, "tp"), P(SP, "tp"),
            P("tp", SP), P("tp", SP), P("tp"), P("tp", None), P(SP, None), P(),
            P(SP, "tp"), P("tp", SP), P(),
        ),
        out_specs=P(("z", "y", "tp"), None),
        check_vma=False,
    )


def solution(mesh):
    return build(mesh, 8, 8)
```

time: 404 us -> 94.7 us (0.23)
  blocking collectives: 182 us -> 0 us
  between operations: 97.8 us -> 0.1 us
  Pallas kernels: 0 us -> 84.6 us
  starting transfers between devices: 48.2 us -> 0 us
  other arithmetic: 20.4 us -> 0 us
  local copies, waits for them, and re-layouts: 23.7 us -> 9.29 us
  loops' own time: 10.2 us -> 0 us
  waiting for transfers between devices: 10.1 us -> 0 us
  matrix products: 9.1 us -> 0 us
    all_gather x8 -> x0, blocking collectives: 122 us -> none  [prefix_by_axis(): pieces = jax.tree.map(lambda part: lax.all_gather(part, axis), subtotal)]
    pallas_call x0 -> x1, Pallas kernels: none -> 84.6 us  [layer(): pl.pallas_call(functools.partial(kernel, sizes), out_shape=jax.ShapeDtype...]
    all_to_all x1 -> x0, starting transfers between devices: 48.2 us -> none  [summed_on_arrival(): lax.all_to_all(cut_along(value, dim, length), axis, 0, 0, tiled=True)]
    unnamed x2 -> x0, blocking collectives: 35.1 us -> none
    all_to_all x2 -> x0, blocking collectives: 25.5 us -> none  [the longest x1 12.8 us: summed_on_arrival(): lax.all_to_all(cut_along(value, dim, length), axis, 0, 0, tiled=True)]
    another operation x2 -> x0, loops' own time: 10.2 us -> none  [summarize(): lax.scan(advance, identity, (decay_total, cell_states, norm_states, peak_...]
    all_to_all x1 -> x0, waiting for transfers between devices: 9.35 us -> none  [summed_on_arrival(): lax.all_to_all(cut_along(value, dim, length), axis, 0, 0, tiled=True)]
    dot_general x12 -> x0, matrix products: 9.1 us -> none  [the longest x1 5.57 us: body(): jnp.dot(hidden, lax.all_gather(down_weight, SP, axis=1, tiled=True), pref...]
  transfers between devices with their start and end apart: 3 -> 0, of which waited for: 1 -> 0; matrix products, arithmetic and copies ran while one was open for 12% -> 0% of each run, Pallas kernels for 0% -> 0%
where the time goes in v1:
time: 94.7 us; the launch traced here: 94 us
  Pallas kernels  84.6 us (89%)
  local copies, waits for them, and re-layouts  9.29 us (10%)
    pallas_call x1, Pallas kernels, layer(): pl.pallas_call(functools.partial(kernel, sizes), out_shape=jax.ShapeDtype...  84.6 us
    unnamed x29, local copies, waits for them, and re-layouts  9.29 us

profile of v1, /device:TPU:1, one launch (start us, length us, event | category | flops | bytes accessed | tf_op | source)
XLA Modules:
  0.0 94.0 jit_solution(7348595362725560072)
XLA Ops:
  0.0 0.0 copy-start.2
  0.0 0.9 copy.16.q2_ref
  0.9 0.0 copy-start.6
  0.9 0.0 copy-start.10
  0.9 0.0 copy-start.11
  0.9 0.0 copy-start.12
  0.9 0.8 copy.17.k2_ref
  1.8 0.0 copy-done.2
  1.8 0.0 copy-done.6
  1.8 0.0 copy-done.10
  1.8 0.0 copy-done.11
  1.8 0.0 copy-done.12
  1.8 0.0 copy-start
  1.8 1.2 %copy-done = bf16[256,2048]{1,0:T(8,128)(2,1)S(1)} copy-done((bf16[256,2048]{1,0:T(8,128)(2,1)S(1)}, bf16[256,2048]{1,0:T(8,128)(2,1)}, u32[]{:S(2)}) %copy-start) | copy-done | bytes 1048600
  3.0 0.0 copy-start.1
  3.0 1.0 %copy-done.1 = bf16[128,2048]{1,0:T(8,128)(2,1)S(1)} copy-done((bf16[128,2048]{1,0:T(8,128)(2,1)S(1)}, bf16[128,2048]{1,0:T(8,128)(2,1)}, u32[]{:S(2)}) %copy-start.1) | copy-done | bytes 524312
  4.1 0.0 copy-start.3
  4.1 0.8 copy-done.3
  4.9 0.0 copy-start.4
  4.9 0.8 copy-done.4
  5.8 0.0 copy-start.5
  5.8 0.8 copy-done.5
  6.6 0.0 copy-start.7
  6.6 0.8 copy-done.7
  7.4 0.0 copy-start.8
  7.4 0.7 copy-done.8
  8.1 0.0 copy-start.9
  8.1 0.7 copy-done.9
  8.8 84.6 %shard_map.145 = bf16[16,2048]{1,0:T(8,128)(2,1)S(1)} custom-call(bf16[128,128]{1,0:T(8,128)(2,1)S(1)} %copy-done.6, bf16[128,128]{1,0:T(8,128)(2,1)S(1)} %copy-done.7, bf16[128,64]{1,0:T(8,128)(2,1)S(1)} %copy.16.q2_ref, bf16[128,64]{1,0:T(8,128)(2,1)S(1)} %copy.17.k2_ref, bf16[128,256]{1,0:T(8,128)(2,1)S(1)} %copy-done.2, bf16[128,256]{1,0:T(8,128)(2,1)S(1)} %copy-done.3, ...), custom_call_target="tpu_custom_call" | custom-call | tf_op jit(solution)/shard_map/pallas_call | solution.py:360
  93.3 0.6 copy.19
Async XLA Ops:
  0.0 1.8 %copy-start.2 = (bf16[128,256]{1,0:T(8,128)(2,1)S(1)}, bf16[128,256]{1,0:T(8,128)(2,1)}, u32[]{:S(2)}) copy-start(bf16[128,256]{1,0:T(8,128)(2,1)} %v_ref.1) | copy-start | bytes 196612
  0.9 0.9 copy-start.6
  0.9 0.9 copy-start.10
  0.9 0.9 copy-start.11
  0.9 0.9 copy-start.12
  1.8 1.2 %copy-start = (bf16[256,2048]{1,0:T(8,128)(2,1)S(1)}, bf16[256,2048]{1,0:T(8,128)(2,1)}, u32[]{:S(2)}) copy-start(bf16[256,2048]{1,0:T(8,128)(2,1)} %ow_ref.1) | copy-start | bytes 3145732
  3.0 1.0 %copy-start.1 = (bf16[128,2048]{1,0:T(8,128)(2,1)S(1)}, bf16[128,2048]{1,0:T(8,128)(2,1)}, u32[]{:S(2)}) copy-start(bf16[128,2048]{1,0:T(8,128)(2,1)} %stream_ref.1) | copy-start | bytes 1572868
  4.1 0.8 copy-start.3
  4.9 0.8 copy-start.4
  5.8 0.8 copy-start.5
  6.6 0.8 copy-start.7
  7.4 0.7 copy-start.8
  8.1 0.7 copy-start.9
